TPU v7x, 32 devices: a whole 2x2x4 slice. The times are simulated.
32 devices in a mesh: ep: 8 (over z, y), tp: 4 (over x, core).
Axes of the slice: x: 2, y: 2, z: 4, core: 2. Of those that a mesh axis runs over, the one named last changes fastest.
Arguments:
- queries: bfloat16 [2048, 8, 128], P('ep', 'tp'), may hold values from -15 to 15
- keys: bfloat16 [2048, 4, 128], P('ep', 'tp'), may hold values from -6 to 6
- values: bfloat16 [2048, 4, 128], P('ep', 'tp'), may hold values from -6 to 6
- key_bias: bfloat16 [2048, 8], P('ep', 'tp'), may hold values from -20 to 2
- out_weight: bfloat16 [1024, 2048], P('tp'), may hold values from -0.1875 to 0.1875
- tokens_b: bfloat16 [4096, 2048], P(('ep', 'tp')), may hold values from -6 to 6
- moe_gain: bfloat16 [2048], replicated, may hold values from 0.099609375 to 1.8984375
- gate_weight: bfloat16 [8, 2048, 2048], P('ep', None, 'tp'), may hold values from -0.125 to 0.125
- up_weight: bfloat16 [8, 2048, 2048], P('ep', None, 'tp'), may hold values from -0.125 to 0.125
- down_weight: bfloat16 [8, 2048, 2048], P('ep', 'tp'), may hold values from -0.125 to 0.125
- routes: int32 [4096, 2], P(('ep', 'tp')), may hold values from 0 to 7, all different within a row; in each aligned block of 128 rows (0 to 127, 128 to 255, ...) at most 48 rows name the same one
- route_weights: float32 [4096, 2], P(('ep', 'tp')), may hold values from 0.2 to 1
Outputs:
- mixed: bfloat16 [2048, 2048], P(('ep', 'tp'))
- moe_out: bfloat16 [4096, 2048], P(('ep', 'tp'))
Inputs may be any that keep to these rules, and one draw needn't show every extreme that they name: `routes`: each row names 2 different experts. In each aligned block of 128 rows (the rows of one device) no expert is named by more than 48 rows, and in some block one expert is named by exactly 48 rows.
All inputs are finite; a program needn't handle non-finite values.
Results may differ from a plain program's by a relative error of at most 0.012.
Values may be sent and summed in bfloat16 or wider, within the bound.
A program may use at most 128 MiB of HBM per device.

v0:
```python
import functools
import math

import jax
import jax.numpy as jnp
from jax import lax
from jax.experimental import pallas as pl
from jax.experimental.pallas import tpu as pltpu
from jax.sharding import PartitionSpec as P

MESH = pl.DeviceIdType.MESH
F32, BF16 = jnp.float32, jnp.bfloat16


def remote(src, dst, send_sem, recv_sem, **where):
    return pltpu.make_async_remote_copy(
        src_ref=src, dst_ref=dst, send_sem=send_sem, recv_sem=recv_sem,
        device_id=where, device_id_type=MESH,
    )


def dot(a, b):
    return jnp.dot(a, b, preferred_element_type=F32)


def columns(rows_ref):
    values = rows_ref[...].astype(F32)
    top, tok = values.shape
    return [
        jnp.transpose(jnp.broadcast_to(values[c : c + 1, :], (128, tok)))[:, 0:1] for c in range(top)
    ]


def slots_of(routes, me, ep, cap):
    tok, top = routes[0].shape[0], len(routes)
    lanes = max(128, -(-ep // 128) * 128)
    lane = lax.broadcasted_iota(jnp.int32, (tok, lanes), 1)
    picks = [(lane == routes[c]).astype(F32) for c in range(top)]
    named = functools.reduce(lambda a, b: a + b, picks)
    row = lax.broadcasted_iota(jnp.int32, (tok, tok), 0)
    col = lax.broadcasted_iota(jnp.int32, (tok, tok), 1)
    earlier = dot((col < row).astype(F32).astype(BF16), named.astype(BF16))
    places = []
    for c in range(top):
        slot = jnp.sum(earlier * picks[c], axis=1, keepdims=True).astype(jnp.int32)
        away = routes[c] - me
        away = jnp.where(away < 0, away + ep, away)
        places.append(away * cap + slot)
    return places


def moe_kernel(
    ep, tp_n, cap, heads,
    routes_ref, weights_ref, tokens_ref, gain_ref, q_ref, keys_ref, values_ref, bias_ref, wo_ref,
    gate_hbm, up_hbm, down_hbm, mixed_ref, out_ref,
    gate, up, down, outbound, rows, core_in, x_in, ret,
    kv, kb, acc, carried, part, mix_core, mix_x,
    w_sem, a_s, a_r, bx_s, bx_r, bc_s, bc_r, bd_s, bd_r,
    p0_s, p0_r, p1_s, p1_r, q_s, q_r, r_s, r_r,
    c_s, cb_s, m_s, mb_s, kv_r, kb_r,
    m0_s, m0_r, m1_s, m1_r, mq_s, mq_r,
):
    me, tp = lax.axis_index("ep"), lax.axis_index("tp")
    mate = tp + 1 - 2 * (tp % 2)
    across = (tp + 2) % 4
    mate_across = (mate + 2) % 4
    beside = me + 1 - 2 * (me % 2)
    span, dim = keys_ref.shape
    tok, width = tokens_ref.shape

    loads = [
        pltpu.make_async_copy(src.at[0], dst, w_sem.at[n])
        for n, (src, dst) in enumerate(((gate_hbm, gate), (up_hbm, up), (down_hbm, down)))
    ]
    for load in loads:
        load.start()

    barrier = pltpu.get_barrier_semaphore()

    def greet(k, _):
        pl.semaphore_signal(barrier, inc=1, device_id={"ep": (me + k) % ep}, device_id_type=MESH)
        return 0

    lax.fori_loop(1, ep, greet, 0)
    for other in (mate, across):
        pl.semaphore_signal(barrier, inc=1, device_id={"tp": other}, device_id_type=MESH)

    kv[me, 0:span] = keys_ref[...]
    kv[me, span : 2 * span] = values_ref[...]
    kb[me] = bias_ref[...]
    acc[...] = jnp.zeros_like(acc)
    carried[...] = jnp.zeros_like(carried)

    places = slots_of([c.astype(jnp.int32) for c in columns(routes_ref)], me, ep, cap)
    slot_id = lax.broadcasted_iota(jnp.int32, (tok, ep * cap), 1)
    hits = [(slot_id == place).astype(F32) for place in places]
    chosen = functools.reduce(lambda a, b: a + b, hits)
    tokens = tokens_ref[...].astype(F32)
    mean = jnp.mean(tokens * tokens, axis=1, keepdims=True)
    normed = (tokens * lax.rsqrt(mean + 1e-06) * gain_ref[...].astype(F32)).astype(BF16)
    packed = dot(jnp.transpose(chosen).astype(BF16), normed).astype(BF16)
    outbound[...] = packed.reshape(ep, cap, width)
    rows[0, tp] = packed[:cap]

    pl.semaphore_wait(barrier, ep + 1)

    def dispatch(k):
        return remote(outbound.at[k], rows.at[k, tp], a_s.at[k], a_r.at[k], ep=(me + k) % ep)

    def relay_across(k):
        return remote(rows.at[k, tp], rows.at[k, tp], bx_s.at[k], bx_r.at[k], tp=across)

    def relay_mate(k):
        return remote(rows.at[k, tp], rows.at[k, tp], bc_s.at[k], bc_r.at[k], tp=mate)

    def relay_both(k):
        return remote(rows.at[k, across], rows.at[k, across], bd_s.at[k], bd_r.at[k], tp=mate)

    def part_mate(k):
        return remote(rows.at[k, mate], core_in.at[k, 0], p0_s.at[k], p0_r.at[k], tp=mate)

    def part_mate_across(k):
        return remote(rows.at[k, mate_across], core_in.at[k, 1], p1_s.at[k], p1_r.at[k], tp=mate)

    def part_across(k):
        return remote(core_in.at[k, 1], x_in.at[k], q_s.at[k], q_r.at[k], tp=across)

    def give_back(k):
        return remote(x_in.at[k], ret.at[k], r_s.at[k], r_r.at[k], ep=(me + ep - k) % ep)

    def along(s):
        return (
            remote(kv.at[s], kv.at[s], c_s.at[s], kv_r.at[s], ep=(me + 2) % ep),
            remote(kb.at[s], kb.at[s], cb_s.at[s], kb_r.at[s], ep=(me + 2) % ep),
        )

    def aside(s):
        return (
            remote(kv.at[s], kv.at[s], m_s.at[s], kv_r.at[s], ep=beside),
            remote(kb.at[s], kb.at[s], mb_s.at[s], kb_r.at[s], ep=beside),
        )

    def pass_keys(j, act):
        s = me - 2 * j

        @pl.when((s >= 0) & (me + 2 < ep))
        def _():
            for copy in along(s):
                act(copy)

        @pl.when((s >= 0) & ((me % 2 == 0) | (j > 0)))
        def _():
            for copy in aside(s):
                act(copy)

    def send(k, _):
        dispatch(k).start()
        return 0

    pass_keys(0, lambda copy: copy.start())

    lax.fori_loop(1, ep, send, 0)

    mix_far = remote(part.at[mate_across], mix_core.at[1], m1_s, m1_r, tp=mate)
    mix_near = remote(part.at[mate], mix_core.at[0], m0_s, m0_r, tp=mate)
    mix_over = remote(mix_core.at[1], mix_x, mq_s, mq_r, tp=across)

    total_rows = heads * span
    nt = (((1,), (1,)), ((), ()))

    def attend(n):
        s = me - n
        key_no = lax.broadcasted_iota(jnp.int32, (total_rows, span), 1)
        query_no = lax.broadcasted_iota(jnp.int32, (total_rows, span), 0) % span
        tri = (
            lax.broadcasted_iota(jnp.int32, (span, span), 0)
            > lax.broadcasted_iota(jnp.int32, (span, span), 1)
        ).astype(F32).astype(BF16)
        bias = kb[s].astype(F32)
        scores = lax.dot_general(q_ref[...], kv[s, 0:span], nt, preferred_element_type=F32)
        scores = scores * (1.0 / math.sqrt(dim)) + jnp.concatenate(
            [jnp.broadcast_to(bias[h : h + 1, :], (span, span)) for h in range(heads)], axis=0
        )
        seen = (key_no < query_no) | (n > 0)
        soft = jnp.log(1.0 + jnp.exp(-jnp.abs(scores)))
        log_take = jnp.minimum(scores, 0.0) - soft
        log_keep = jnp.where(seen, log_take - scores, 0.0)
        high = log_keep.astype(BF16)
        low = (log_keep - high.astype(F32)).astype(BF16)
        after = dot(high, tri) + dot(low, tri)
        before = carried[:, 0:1]
        stick = jnp.where(seen, jnp.exp(log_take + after + before), 0.0).astype(BF16)
        acc[...] += dot(stick, kv[s, span : 2 * span])
        carried[...] = jnp.broadcast_to(
            before + jnp.sum(log_keep, axis=1, keepdims=True), carried.shape
        )

    def project():
        mixed = functools.reduce(
            lambda a, b: a + b,
            [
                dot(acc[h * span : (h + 1) * span].astype(BF16), wo_ref[h * dim : (h + 1) * dim, :])
                for h in range(heads)
            ],
        )
        part[...] = mixed.astype(BF16).reshape(part.shape)

    def step(i, _):
        @pl.when(i < ep)
        def _():
            @pl.when(i > 0)
            def _():
                dispatch(i).wait_recv()

            relay_across(i).start()
            relay_mate(i).start()

        @pl.when((i >= 1) & (me - 2 * i >= 0))
        def _():
            for copy in along(me - 2 * i):
                copy.wait_recv()
            pass_keys(i, lambda copy: copy.start())

        @pl.when((i >= 1) & (i < ep + 1))
        def _():
            k = i - 1
            relay_across(k).wait_recv()
            relay_both(k).start()

        @pl.when((i >= 3) & (i < ep + 3))
        def _():
            k = i - 3
            part_mate(k).wait()
            part_mate_across(k).wait()
            core_in[k, 1] = (core_in[k, 1].astype(F32) + rows[k, across].astype(F32)).astype(BF16)
            part_across(k).start()

        @pl.when((i >= 2) & (i < ep + 2))
        def _():
            k = i - 2

            @pl.when(i == 2)
            def _():
                for load in loads:
                    load.wait()

            relay_mate(k).wait()
            relay_both(k).wait()
            relay_across(k).wait_send()
            x = rows[k].reshape(tp_n * cap, width)
            gated = dot(x, gate[...])
            lifted = dot(x, up[...])
            hidden = (gated / (1.0 + jnp.exp(-gated)) * lifted).astype(BF16)
            rows[k] = dot(hidden, down[...]).astype(BF16).reshape(tp_n, cap, width)
            part_mate(k).start()
            part_mate_across(k).start()

        @pl.when((i >= 2) & (i - 2 <= me))
        def _():
            n = i - 2

            @pl.when(n % 2 == 1)
            def _():
                for copy in aside(me - n):
                    copy.wait_recv()

            attend(n)

        @pl.when(i == ep + 2)
        def _():
            project()
            mix_far.start()
            mix_near.start()

        @pl.when(i == ep + 3)
        def _():
            mix_far.wait()
            mix_core[1] = (mix_core[1].astype(F32) + part[across].astype(F32)).astype(BF16)
            mix_over.start()

        @pl.when(i >= 4)
        def _():
            k = i - 4
            part_across(k).wait()
            total = (
                rows[k, tp].astype(F32) + core_in[k, 0].astype(F32) + x_in[k].astype(F32)
            ).astype(BF16)

            @pl.when(k > 0)
            def _():
                x_in[k] = total
                give_back(k).start()

            @pl.when(k == 0)
            def _():
                ret[0] = total

        return 0

    lax.fori_loop(0, ep + 4, step, 0)

    def drain(j, _):
        pass_keys(j, lambda copy: copy.wait_send())
        return 0

    lax.fori_loop(0, ep // 2, drain, 0)
    mix_near.wait()
    mix_over.wait()
    mixed_ref[...] = (
        part[tp].astype(F32) + mix_core[0].astype(F32) + mix_x[...].astype(F32)
    ).astype(BF16)

    def finish(k, _):
        dispatch(k).wait_send()
        give_back(k).wait()
        return 0

    lax.fori_loop(1, ep, finish, 0)
    weights = columns(weights_ref)
    mix = functools.reduce(
        lambda a, b: a + b, [hit * weights[c] for c, hit in enumerate(hits)]
    )
    high = mix.astype(BF16)
    low = (mix - high.astype(F32)).astype(BF16)
    results = ret[...].reshape(ep * cap, width)
    out_ref[...] = (dot(high, results) + dot(low, results)).astype(BF16)


def body(
    queries, keys, values, key_bias, out_weight, tokens_b, moe_gain,
    gate_weight, up_weight, down_weight, routes, route_weights,
):
    ep, tp_n = lax.axis_size("ep"), lax.axis_size("tp")
    tok, width = tokens_b.shape
    top = routes.shape[1]
    units = gate_weight.shape[2]
    experts = ep * gate_weight.shape[0]
    capacity = max(2, 3 * top * tok // (2 * experts))
    cap = -(-capacity // 16) * 16
    span, heads, dim = queries.shape
    share = span // tp_n
    vmem = pl.BlockSpec(memory_space=pltpu.VMEM)
    hbm = pl.BlockSpec(memory_space=pl.ANY)
    dma = pltpu.SemaphoreType.DMA
    return pl.pallas_call(
        functools.partial(moe_kernel, ep, tp_n, cap, heads),
        out_shape=(
            jax.ShapeDtypeStruct((share, width), BF16),
            jax.ShapeDtypeStruct((tok, width), BF16),
        ),
        in_specs=[vmem] * 9 + [hbm] * 3,
        out_specs=(vmem, vmem),
        scratch_shapes=[
            pltpu.VMEM((width, units), BF16),
            pltpu.VMEM((width, units), BF16),
            pltpu.VMEM((units, width), BF16),
            pltpu.VMEM((ep, cap, width), BF16),
            pltpu.VMEM((ep, tp_n, cap, width), BF16),
            pltpu.VMEM((ep, 2, cap, width), BF16),
            pltpu.VMEM((ep, cap, width), BF16),
            pltpu.VMEM((ep, cap, width), BF16),
            pltpu.VMEM((ep, 2 * span, dim), BF16),
            pltpu.VMEM((ep, heads, span), BF16),
            pltpu.VMEM((heads * span, dim), F32),
            pltpu.VMEM((heads * span, 128), F32),
            pltpu.VMEM((tp_n, share, width), BF16),
            pltpu.VMEM((2, share, width), BF16),
            pltpu.VMEM((share, width), BF16),
            dma((3,)),
        ] + [dma((ep,))] * 22 + [dma] * 6,
        compiler_params=pltpu.CompilerParams(
            collective_id=0, has_side_effects=True, vmem_limit_bytes=67043328
        ),
        cost_estimate=pl.CostEstimate(
            flops=6 * ep * tp_n * cap * width * units, bytes_accessed=6 * width * units,
            transcendentals=0,
        ),
        name="layer",
    )(
        jnp.transpose(routes), jnp.transpose(route_weights), tokens_b, moe_gain.reshape(1, width),
        jnp.transpose(queries, (1, 0, 2)).reshape(heads * span, dim),
        keys[:, 0], values[:, 0], jnp.transpose(key_bias), out_weight,
        gate_weight, up_weight, down_weight,
    )


def solution(mesh):
    in_specs = (
        P("ep", "tp", None),
        P("ep", "tp", None),
        P("ep", "tp", None),
        P("ep", "tp"),
        P("tp", None),
        P(("ep", "tp"), None),
        P(),
        P("ep", None, "tp"),
        P("ep", None, "tp"),
        P("ep", "tp", None),
        P(("ep", "tp"), None),
        P(("ep", "tp"), None),
    )
    out_specs = (P(("ep", "tp"), None), P(("ep", "tp"), None))
    return jax.shard_map(body, mesh=mesh, in_specs=in_specs, out_specs=out_specs, check_vma=False)
```

profile of v0, /device:TPU:0, one launch (start us, length us, event | category | flops | bytes accessed | tf_op | source)
XLA Modules:
  0.0 128.2 jit_solution(14515395574440116965)
XLA Ops:
  0.6 1.3 %reshape.10.gain_ref = bf16[1,2048]{1,0:T(2,128)(2,1)} reshape(bf16[2048]{0:T(1024)(128)(2,1)} %param.18) | data formatting | bytes 8192 | tf_op jit(solution)/shard_map/reshape | solution.py:380
  1.9 1.6 %copy.14 = bf16[2,256,128]{2,1,0:T(8,128)(2,1)} copy(bf16[2,256,128]{2,0,1:T(2,128)(2,1)} %bitcast.7) | data formatting | bytes 262144 | tf_op jit(solution)/shard_map/transpose | solution.py:381
  3.5 121.1 %layer.1 = (bf16[64,2048]{1,0:T(8,128)(2,1)}, bf16[128,2048]{1,0:T(8,128)(2,1)}) custom-call(s32[2,128]{1,0:T(2,128)} %bitcast.11, f32[2,128]{1,0:T(2,128)} %bitcast.12, bf16[128,2048]{1,0:T(8,128)(2,1)} %tokens_ref.1, bf16[1,2048]{1,0:T(2,128)(2,1)} %reshape.10.gain_ref, bf16[512,128]{1,0:T(8,128)(2,1)} %bitcast.8, bf16[256,128]{1,0:T(8,128)(2,1)} %bitcast.9, ...), custom_call_target="tpu_custom_call" | custom-call | flops 9663676416 | bytes 6291456 | tf_op jit(solution)/shard_map/layer/pallas_call | solution.py:345
  124.6 1.7 %copy.17 = bf16[64,2048]{1,0:T(8,128)(2,1)} copy(bf16[64,2048]{1,0:T(8,128)(2,1)} %get-tuple-element.4) | data formatting | bytes 524288
  126.3 1.9 %copy.18 = bf16[128,2048]{1,0:T(8,128)(2,1)} copy(bf16[128,2048]{1,0:T(8,128)(2,1)} %get-tuple-element.5) | data formatting | bytes 1048576
where the time goes:
time: 128 us
  Pallas kernels  121 us (95%)
  local copies, waits for them, and re-layouts  6.42 us (5%)
    pallas_call x1, Pallas kernels, body(): pl.pallas_call(functools.partial(moe_kernel, ep, tp_n, cap, heads), out_s...  121 us
    unnamed x2, local copies, waits for them, and re-layouts  3.55 us

commit v1 on v0

--- a/solution.py
+++ b/solution.py
@@ -11,6 +11,20 @@
 MESH = pl.DeviceIdType.MESH
 F32, BF16 = jnp.float32, jnp.bfloat16
 
+SLOTS = 34
+SENDS = ((5, 1, 4, 3, 6, 2, 7), (4, 3, 7, 2, 1, 5, 6))
+PLAN = {
+    'part': ((0, 5505024, 16805888, 2622976, 3), (0, 1441792, 262149, 7350272, 768)),
+    'fin': ((0, 0, 72351744, 6320128, 12584), (0, 0, 1536, 336, 3612744)),
+    'dot': ((0, 33574977, 526080, 12294, 0), (0, 266326, 131120, 28680, 0)),
+    'relay': ((55706640, 526080, 96, 0, 0), (271713, 2096, 28672, 0, 0)),
+    'both': ((4198400, 2293840, 100665351, 0, 0), (90177536, 50463760, 134217728, 112, 0)),
+    'kvf': ((1, 33554432, 0, 262192, 0), (65536, 0, 770, 4, 0)),
+    'att': ((256, 0, 204800, 141952260, 0), (0, 1048576, 4390944, 141971456, 0)),
+    'mix1': ((0, 0, 0, 0, 1), (0, 0, 0, 0, 256)),
+    'mix2': ((0, 0, 0, 0, 1), (0, 0, 0, 0, 256)),
+}
+
 
 def remote(src, dst, send_sem, recv_sem, **where):
     return pltpu.make_async_remote_copy(
@@ -21,6 +35,15 @@
 
 def dot(a, b):
     return jnp.dot(a, b, preferred_element_type=F32)
+
+
+def flip(a, b, n):
+    out, bit = 0, 1
+    while bit < n:
+        p, q = (a // bit) % 2, (b // bit) % 2
+        out = out + bit * (p + q - 2 * p * q)
+        bit *= 2
+    return out
 
 
 def columns(rows_ref):
@@ -43,9 +66,7 @@
     places = []
     for c in range(top):
         slot = jnp.sum(earlier * picks[c], axis=1, keepdims=True).astype(jnp.int32)
-        away = routes[c] - me
-        away = jnp.where(away < 0, away + ep, away)
-        places.append(away * cap + slot)
+        places.append((routes[c] ^ me) * cap + slot)
     return places
 
 
@@ -65,6 +86,7 @@
     across = (tp + 2) % 4
     mate_across = (mate + 2) % 4
     beside = me + 1 - 2 * (me % 2)
+    place = ((me // 2 + 1) // 2) % 2
     span, dim = keys_ref.shape
     tok, width = tokens_ref.shape
 
@@ -104,8 +126,39 @@
 
     pl.semaphore_wait(barrier, ep + 1)
 
+    planned = ep == 8
+
+    def pick(choices, n):
+        value = choices[-1]
+        for c in range(len(choices) - 1):
+            value = jnp.where(n == c, choices[c], value)
+        return value
+
+    def plan(i):
+        if planned:
+            word, digit = i // 7, 4 * (i % 7)
+            work = {}
+            for stage, table in PLAN.items():
+                packed = pick([pick(row, place) for row in zip(*table)], word)
+                entry = (packed >> digit) & 15
+                work[stage] = (entry > 0, entry - 1)
+            return work
+
+        def lagged(lag):
+            return (i >= lag) & (i < ep + lag), i - lag
+
+        def turned(lag):
+            active, p = lagged(lag)
+            return active, jnp.where(p < ep - 2, p + 2, ep - 1 - p)
+
+        return {
+            "part": turned(5), "fin": turned(6), "dot": lagged(2), "relay": lagged(0),
+            "both": lagged(1), "kvf": ((i == 0) | (i % 2 == 1), (i + 1) // 2), "att": lagged(2),
+            "mix1": (i == ep + 2, 0), "mix2": (i == ep + 3, 0),
+        }
+
     def dispatch(k):
-        return remote(outbound.at[k], rows.at[k, tp], a_s.at[k], a_r.at[k], ep=(me + k) % ep)
+        return remote(outbound.at[k], rows.at[k, tp], a_s.at[k], a_r.at[k], ep=flip(me, k, ep))
 
     def relay_across(k):
         return remote(rows.at[k, tp], rows.at[k, tp], bx_s.at[k], bx_r.at[k], tp=across)
@@ -126,7 +179,7 @@
         return remote(core_in.at[k, 1], x_in.at[k], q_s.at[k], q_r.at[k], tp=across)
 
     def give_back(k):
-        return remote(x_in.at[k], ret.at[k], r_s.at[k], r_r.at[k], ep=(me + ep - k) % ep)
+        return remote(x_in.at[k], ret.at[k], r_s.at[k], r_r.at[k], ep=flip(me, k, ep))
 
     def along(s):
         return (
@@ -153,13 +206,15 @@
             for copy in aside(s):
                 act(copy)
 
-    def send(k, _):
-        dispatch(k).start()
-        return 0
-
-    pass_keys(0, lambda copy: copy.start())
-
-    lax.fori_loop(1, ep, send, 0)
+    if planned:
+        for turn in zip(*SENDS):
+            dispatch(pick(turn, place)).start()
+    else:
+        def send(k, _):
+            dispatch(k).start()
+            return 0
+
+        lax.fori_loop(1, ep, send, 0)
 
     mix_far = remote(part.at[mate_across], mix_core.at[1], m1_s, m1_r, tp=mate)
     mix_near = remote(part.at[mate], mix_core.at[0], m0_s, m0_r, tp=mate)
@@ -206,44 +261,36 @@
         part[...] = mixed.astype(BF16).reshape(part.shape)
 
     def step(i, _):
-        @pl.when(i < ep)
-        def _():
-            @pl.when(i > 0)
-            def _():
-                dispatch(i).wait_recv()
-
-            relay_across(i).start()
-            relay_mate(i).start()
-
-        @pl.when((i >= 1) & (me - 2 * i >= 0))
-        def _():
-            for copy in along(me - 2 * i):
-                copy.wait_recv()
-            pass_keys(i, lambda copy: copy.start())
-
-        @pl.when((i >= 1) & (i < ep + 1))
-        def _():
-            k = i - 1
-            relay_across(k).wait_recv()
-            relay_both(k).start()
-
-        @pl.when((i >= 3) & (i < ep + 3))
-        def _():
-            k = i - 3
+        work = plan(i)
+
+        @pl.when(work["part"][0])
+        def _():
+            k = work["part"][1]
             part_mate(k).wait()
             part_mate_across(k).wait()
             core_in[k, 1] = (core_in[k, 1].astype(F32) + rows[k, across].astype(F32)).astype(BF16)
             part_across(k).start()
 
-        @pl.when((i >= 2) & (i < ep + 2))
-        def _():
-            k = i - 2
-
-            @pl.when(i == 2)
+        @pl.when(work["fin"][0])
+        def _():
+            k = work["fin"][1]
+            part_across(k).wait()
+            total = (
+                rows[k, tp].astype(F32) + core_in[k, 0].astype(F32) + x_in[k].astype(F32)
+            ).astype(BF16)
+
+            @pl.when(k > 0)
             def _():
-                for load in loads:
-                    load.wait()
-
+                x_in[k] = total
+                give_back(k).start()
+
+            @pl.when(k == 0)
+            def _():
+                ret[0] = total
+
+        @pl.when(work["dot"][0])
+        def _():
+            k = work["dot"][1]
             relay_mate(k).wait()
             relay_both(k).wait()
             relay_across(k).wait_send()
@@ -255,9 +302,37 @@
             part_mate(k).start()
             part_mate_across(k).start()
 
-        @pl.when((i >= 2) & (i - 2 <= me))
-        def _():
-            n = i - 2
+        @pl.when(work["relay"][0])
+        def _():
+            k = work["relay"][1]
+
+            @pl.when(k > 0)
+            def _():
+                dispatch(k).wait_recv()
+
+            relay_across(k).start()
+            relay_mate(k).start()
+
+        @pl.when(work["both"][0])
+        def _():
+            k = work["both"][1]
+            relay_across(k).wait_recv()
+            relay_both(k).start()
+
+        @pl.when(work["kvf"][0] & (me - 2 * work["kvf"][1] >= 0))
+        def _():
+            j = work["kvf"][1]
+
+            @pl.when(j > 0)
+            def _():
+                for copy in along(me - 2 * j):
+                    copy.wait_recv()
+
+            pass_keys(j, lambda copy: copy.start())
+
+        @pl.when(work["att"][0] & (work["att"][1] <= me))
+        def _():
+            n = work["att"][1]
 
             @pl.when(n % 2 == 1)
             def _():
@@ -266,38 +341,23 @@
 
             attend(n)
 
-        @pl.when(i == ep + 2)
+        @pl.when(work["mix1"][0])
         def _():
             project()
             mix_far.start()
             mix_near.start()
 
-        @pl.when(i == ep + 3)
+        @pl.when(work["mix2"][0])
         def _():
             mix_far.wait()
             mix_core[1] = (mix_core[1].astype(F32) + part[across].astype(F32)).astype(BF16)
             mix_over.start()
 
-        @pl.when(i >= 4)
-        def _():
-            k = i - 4
-            part_across(k).wait()
-            total = (
-                rows[k, tp].astype(F32) + core_in[k, 0].astype(F32) + x_in[k].astype(F32)
-            ).astype(BF16)
-
-            @pl.when(k > 0)
-            def _():
-                x_in[k] = total
-                give_back(k).start()
-
-            @pl.when(k == 0)
-            def _():
-                ret[0] = total
-
         return 0
 
-    lax.fori_loop(0, ep + 4, step, 0)
+    for load in loads:
+        load.wait()
+    lax.fori_loop(0, SLOTS if planned else ep + 6, step, 0)
 
     def drain(j, _):
         pass_keys(j, lambda copy: copy.wait_send())

time: 128 us -> 100 us (0.78)
  Pallas kernels: 121 us -> 92.4 us
    pallas_call x1, Pallas kernels: 121 us -> 92.4 us  [body(): pl.pallas_call(functools.partial(moe_kernel, ep, tp_n, cap, heads), out_s...]
where the time goes in v1:
time: 100 us; the launch traced here: 99.5 us
  Pallas kernels  92.4 us (92%)
  local copies, waits for them, and re-layouts  6.42 us (6%)
    pallas_call x1, Pallas kernels, body(): pl.pallas_call(functools.partial(moe_kernel, ep, tp_n, cap, heads), out_s...  92.4 us
    unnamed x2, local copies, waits for them, and re-layouts  3.55 us

profile of v1, /device:TPU:0, one launch (start us, length us, event | category | flops | bytes accessed | tf_op | source)
XLA Modules:
  0.0 99.5 jit_solution(64427740547943599)
XLA Ops:
  0.6 1.3 %reshape.10.gain_ref = bf16[1,2048]{1,0:T(2,128)(2,1)} reshape(bf16[2048]{0:T(1024)(128)(2,1)} %param.18) | data formatting | bytes 8192 | tf_op jit(solution)/shard_map/reshape | solution.py:440
  1.9 1.6 %copy.14 = bf16[2,256,128]{2,1,0:T(8,128)(2,1)} copy(bf16[2,256,128]{2,0,1:T(2,128)(2,1)} %bitcast.7) | data formatting | bytes 262144 | tf_op jit(solution)/shard_map/transpose | solution.py:441
  3.5 92.4 %layer.1 = (bf16[64,2048]{1,0:T(8,128)(2,1)}, bf16[128,2048]{1,0:T(8,128)(2,1)}) custom-call(s32[2,128]{1,0:T(2,128)} %bitcast.11, f32[2,128]{1,0:T(2,128)} %bitcast.12, bf16[128,2048]{1,0:T(8,128)(2,1)} %tokens_ref.1, bf16[1,2048]{1,0:T(2,128)(2,1)} %reshape.10.gain_ref, bf16[512,128]{1,0:T(8,128)(2,1)} %bitcast.8, bf16[256,128]{1,0:T(8,128)(2,1)} %bitcast.9, ...), custom_call_target="tpu_custom_call" | custom-call | flops 9663676416 | bytes 6291456 | tf_op jit(solution)/shard_map/layer/pallas_call | solution.py:405
  95.9 1.7 %copy.17 = bf16[64,2048]{1,0:T(8,128)(2,1)} copy(bf16[64,2048]{1,0:T(8,128)(2,1)} %get-tuple-element.4) | data formatting | bytes 524288
  97.6 1.9 %copy.18 = bf16[128,2048]{1,0:T(8,128)(2,1)} copy(bf16[128,2048]{1,0:T(8,128)(2,1)} %get-tuple-element.5) | data formatting | bytes 1048576

commit v2 on v1

--- a/solution.py
+++ b/solution.py
@@ -12,17 +12,17 @@
 F32, BF16 = jnp.float32, jnp.bfloat16
 
 SLOTS = 34
-SENDS = ((5, 1, 4, 3, 6, 2, 7), (4, 3, 7, 2, 1, 5, 6))
+SENDS = ((6, 4, 3, 2, 1, 5, 7), (1, 5, 6, 7, 2, 3, 4))
 PLAN = {
-    'part': ((0, 5505024, 16805888, 2622976, 3), (0, 1441792, 262149, 7350272, 768)),
-    'fin': ((0, 0, 72351744, 6320128, 12584), (0, 0, 1536, 336, 3612744)),
-    'dot': ((0, 33574977, 526080, 12294, 0), (0, 266326, 131120, 28680, 0)),
-    'relay': ((55706640, 526080, 96, 0, 0), (271713, 2096, 28672, 0, 0)),
-    'both': ((4198400, 2293840, 100665351, 0, 0), (90177536, 50463760, 134217728, 112, 0)),
-    'kvf': ((1, 33554432, 0, 262192, 0), (65536, 0, 770, 4, 0)),
-    'att': ((256, 0, 204800, 141952260, 0), (0, 1048576, 4390944, 141971456, 0)),
-    'mix1': ((0, 0, 0, 0, 1), (0, 0, 0, 0, 256)),
-    'mix2': ((0, 0, 0, 0, 1), (0, 0, 0, 0, 256)),
+    'part': ((0, 100663298, 138413824, 1246464, 0), (0, 6619136, 262256, 3146368, 4096)),
+    'fin': ((0, 0, 24576, 42205296, 4869), (0, 0, 100663301, 67108976, 1245824)),
+    'dot': ((131072, 4587536, 2055, 12293, 0), (0, 117834757, 8519680, 77824, 0)),
+    'relay': ((73414433, 128, 80, 0, 0), (57099553, 524288, 0, 0, 0)),
+    'both': ((66048, 29510, 327808, 0, 0), (20480, 30272, 98816, 768, 0)),
+    'kvf': ((0, 256, 50331650, 1024, 0), (16, 2097152, 262192, 0, 0)),
+    'att': ((0, 16777216, 8192, 105923328, 135), (0, 1, 33554432, 105907203, 32775)),
+    'mix1': ((0, 0, 0, 0, 16), (0, 0, 0, 0, 4096)),
+    'mix2': ((0, 0, 0, 0, 16), (0, 0, 0, 0, 65536)),
 }
 
 
@@ -75,7 +75,7 @@
     routes_ref, weights_ref, tokens_ref, gain_ref, q_ref, keys_ref, values_ref, bias_ref, wo_ref,
     gate_hbm, up_hbm, down_hbm, mixed_ref, out_ref,
     gate, up, down, outbound, rows, core_in, x_in, ret,
-    kv, kb, acc, carried, part, mix_core, mix_x,
+    qs, kv, kb, acc, carried, part, mix_core, mix_x,
     w_sem, a_s, a_r, bx_s, bx_r, bc_s, bc_r, bd_s, bd_r,
     p0_s, p0_r, p1_s, p1_r, q_s, q_r, r_s, r_r,
     c_s, cb_s, m_s, mb_s, kv_r, kb_r,
@@ -110,6 +110,9 @@
     kv[me, 0:span] = keys_ref[...]
     kv[me, span : 2 * span] = values_ref[...]
     kb[me] = bias_ref[...]
+    wide = q_ref[...].astype(F32)
+    for h in range(heads):
+        qs[h * span : (h + 1) * span] = wide[:, h, :].astype(BF16)
     acc[...] = jnp.zeros_like(acc)
     carried[...] = jnp.zeros_like(carried)
 
@@ -119,7 +122,7 @@
     chosen = functools.reduce(lambda a, b: a + b, hits)
     tokens = tokens_ref[...].astype(F32)
     mean = jnp.mean(tokens * tokens, axis=1, keepdims=True)
-    normed = (tokens * lax.rsqrt(mean + 1e-06) * gain_ref[...].astype(F32)).astype(BF16)
+    normed = (tokens * lax.rsqrt(mean + 1e-06) * gain_ref[...].astype(F32).reshape(1, width)).astype(BF16)
     packed = dot(jnp.transpose(chosen).astype(BF16), normed).astype(BF16)
     outbound[...] = packed.reshape(ep, cap, width)
     rows[0, tp] = packed[:cap]
@@ -232,7 +235,7 @@
             > lax.broadcasted_iota(jnp.int32, (span, span), 1)
         ).astype(F32).astype(BF16)
         bias = kb[s].astype(F32)
-        scores = lax.dot_general(q_ref[...], kv[s, 0:span], nt, preferred_element_type=F32)
+        scores = lax.dot_general(qs[...], kv[s, 0:span], nt, preferred_element_type=F32)
         scores = scores * (1.0 / math.sqrt(dim)) + jnp.concatenate(
             [jnp.broadcast_to(bias[h : h + 1, :], (span, span)) for h in range(heads)], axis=0
         )
@@ -419,6 +422,7 @@
             pltpu.VMEM((ep, 2, cap, width), BF16),
             pltpu.VMEM((ep, cap, width), BF16),
             pltpu.VMEM((ep, cap, width), BF16),
+            pltpu.VMEM((heads * span, dim), BF16),
             pltpu.VMEM((ep, 2 * span, dim), BF16),
             pltpu.VMEM((ep, heads, span), BF16),
             pltpu.VMEM((heads * span, dim), F32),
@@ -437,8 +441,8 @@
         ),
         name="layer",
     )(
-        jnp.transpose(routes), jnp.transpose(route_weights), tokens_b, moe_gain.reshape(1, width),
-        jnp.transpose(queries, (1, 0, 2)).reshape(heads * span, dim),
+        jnp.transpose(routes), jnp.transpose(route_weights), tokens_b, moe_gain,
+        queries,
         keys[:, 0], values[:, 0], jnp.transpose(key_bias), out_weight,
         gate_weight, up_weight, down_weight,
     )

time: 100 us -> 92.8 us (0.928)
  Pallas kernels: 92.4 us -> 88.4 us
  local copies, waits for them, and re-layouts: 6.42 us -> 3.55 us
    pallas_call x1, Pallas kernels: 92.4 us -> 88.4 us  [body(): pl.pallas_call(functools.partial(moe_kernel, ep, tp_n, cap, heads), out_s...]
    transpose x1 -> x0, local copies, waits for them, and re-layouts: 1.58 us -> none  [body(): jnp.transpose(queries, (1, 0, 2)).reshape(heads * span, dim)]
    reshape x1 -> x0, local copies, waits for them, and re-layouts: 1.29 us -> none  [body(): moe_gain.reshape(1, width)]
where the time goes in v2:
time: 92.8 us; the launch traced here: 92.6 us
  Pallas kernels  88.4 us (95%)
  local copies, waits for them, and re-layouts  3.55 us (4%)
    pallas_call x1, Pallas kernels, body(): pl.pallas_call(functools.partial(moe_kernel, ep, tp_n, cap, heads), out_s...  88.4 us
    unnamed x2, local copies, waits for them, and re-layouts  3.55 us

profile of v2, /device:TPU:0, one launch (start us, length us, event | category | flops | bytes accessed | tf_op | source)
XLA Modules:
  0.0 92.6 jit_solution(10411730971714227021)
XLA Ops:
  0.6 88.4 %layer.1 = (bf16[64,2048]{1,0:T(8,128)(2,1)}, bf16[128,2048]{1,0:T(8,128)(2,1)}) custom-call(s32[2,128]{1,0:T(2,128)} %bitcast.7, f32[2,128]{1,0:T(2,128)} %bitcast.8, bf16[128,2048]{1,0:T(8,128)(2,1)} %tokens_ref.1, bf16[2048]{0:T(1024)(128)(2,1)} %gain_ref.1, bf16[256,2,128]{2,1,0:T(2,128)(2,1)} %q_ref.1, bf16[256,128]{1,0:T(8,128)(2,1)} %bitcast.5, ...), custom_call_target="tpu_custom_call" | custom-call | flops 9663676416 | bytes 6291456 | tf_op jit(solution)/shard_map/layer/pallas_call | solution.py:408
  89.0 1.7 %copy.16 = bf16[64,2048]{1,0:T(8,128)(2,1)} copy(bf16[64,2048]{1,0:T(8,128)(2,1)} %get-tuple-element.4) | data formatting | bytes 524288
  90.7 1.9 %copy.17 = bf16[128,2048]{1,0:T(8,128)(2,1)} copy(bf16[128,2048]{1,0:T(8,128)(2,1)} %get-tuple-element.5) | data formatting | bytes 1048576

commit v3 on v2

--- a/solution.py
+++ b/solution.py
@@ -11,18 +11,18 @@
 MESH = pl.DeviceIdType.MESH
 F32, BF16 = jnp.float32, jnp.bfloat16
 
-SLOTS = 34
-SENDS = ((6, 4, 3, 2, 1, 5, 7), (1, 5, 6, 7, 2, 3, 4))
+SLOTS = 36
+SENDS = ((6, 4, 3, 2, 1, 5, 7), (6, 1, 2, 5, 3, 7, 4))
 PLAN = {
-    'part': ((0, 100663298, 138413824, 1246464, 0), (0, 6619136, 262256, 3146368, 4096)),
-    'fin': ((0, 0, 24576, 42205296, 4869), (0, 0, 100663301, 67108976, 1245824)),
-    'dot': ((131072, 4587536, 2055, 12293, 0), (0, 117834757, 8519680, 77824, 0)),
-    'relay': ((73414433, 128, 80, 0, 0), (57099553, 524288, 0, 0, 0)),
-    'both': ((66048, 29510, 327808, 0, 0), (20480, 30272, 98816, 768, 0)),
-    'kvf': ((0, 256, 50331650, 1024, 0), (16, 2097152, 262192, 0, 0)),
-    'att': ((0, 16777216, 8192, 105923328, 135), (0, 1, 33554432, 105907203, 32775)),
-    'mix1': ((0, 0, 0, 0, 16), (0, 0, 0, 0, 4096)),
-    'mix2': ((0, 0, 0, 0, 16), (0, 0, 0, 0, 65536)),
+    'part': ((0, 6291568, 136331264, 5242880, 304, 0), (0, 458752, 72744992, 25165827, 0, 0)),
+    'fin': ((0, 0, 460288, 262144, 50667648, 1), (0, 0, 28672, 329248, 25362496, 0)),
+    'dot': ((2162688, 393223, 32832, 13568, 0, 0), (0, 38825984, 3163648, 32769, 0, 0)),
+    'relay': ((67122977, 32774, 5, 0, 0, 0), (55005712, 1536, 8, 0, 0, 0)),
+    'both': ((7348480, 58721856, 0, 5, 0, 0), (117440512, 101711954, 52, 2048, 0, 0)),
+    'kvf': ((1048576, 512, 50331648, 64, 0, 0), (1, 0, 12320, 67108864, 0, 0)),
+    'att': ((0, 1, 0, 70254594, 8848901, 0), (0, 65536, 0, 67305984, 34661, 0)),
+    'mix1': ((0, 0, 0, 0, 1048576, 0), (0, 0, 0, 0, 65536, 0)),
+    'mix2': ((0, 0, 0, 0, 1048576, 0), (0, 0, 0, 0, 65536, 0)),
 }
 
 
@@ -72,9 +72,9 @@
 
 def moe_kernel(
     ep, tp_n, cap, heads,
-    routes_ref, weights_ref, tokens_ref, gain_ref, q_ref, keys_ref, values_ref, bias_ref, wo_ref,
+    routes_ref, weights_ref, tokens_ref, gain_ref, q_ref, keys_ref, values_ref, bias_ref, wo_hbm,
     gate_hbm, up_hbm, down_hbm, mixed_ref, out_ref,
-    gate, up, down, outbound, rows, core_in, x_in, ret,
+    wo_ref, gate, up, down, outbound, rows, core_in, x_in, ret,
     qs, kv, kb, acc, carried, part, mix_core, mix_x,
     w_sem, a_s, a_r, bx_s, bx_r, bc_s, bc_r, bd_s, bd_r,
     p0_s, p0_r, p1_s, p1_r, q_s, q_r, r_s, r_r,
@@ -91,8 +91,10 @@
     tok, width = tokens_ref.shape
 
     loads = [
-        pltpu.make_async_copy(src.at[0], dst, w_sem.at[n])
-        for n, (src, dst) in enumerate(((gate_hbm, gate), (up_hbm, up), (down_hbm, down)))
+        pltpu.make_async_copy(src, dst, w_sem.at[n])
+        for n, (src, dst) in enumerate(
+            ((gate_hbm.at[0], gate), (up_hbm.at[0], up), (down_hbm.at[0], down), (wo_hbm, wo_ref))
+        )
     ]
     for load in loads:
         load.start()
@@ -411,9 +413,10 @@
             jax.ShapeDtypeStruct((share, width), BF16),
             jax.ShapeDtypeStruct((tok, width), BF16),
         ),
-        in_specs=[vmem] * 9 + [hbm] * 3,
+        in_specs=[vmem] * 8 + [hbm] * 4,
         out_specs=(vmem, vmem),
         scratch_shapes=[
+            pltpu.VMEM((heads * dim, width), BF16),
             pltpu.VMEM((width, units), BF16),
             pltpu.VMEM((width, units), BF16),
             pltpu.VMEM((units, width), BF16),
@@ -430,7 +433,7 @@
             pltpu.VMEM((tp_n, share, width), BF16),
             pltpu.VMEM((2, share, width), BF16),
             pltpu.VMEM((share, width), BF16),
-            dma((3,)),
+            dma((4,)),
         ] + [dma((ep,))] * 22 + [dma] * 6,
         compiler_params=pltpu.CompilerParams(
             collective_id=0, has_side_effects=True, vmem_limit_bytes=67043328

time: 92.8 us -> 90.3 us (0.973)
  Pallas kernels: 88.4 us -> 85.9 us
    pallas_call x1, Pallas kernels: 88.4 us -> 85.9 us  [body(): pl.pallas_call(functools.partial(moe_kernel, ep, tp_n, cap, heads), out_s...]
where the time goes in v3:
time: 90.3 us; the launch traced here: 90.1 us
  Pallas kernels  85.9 us (95%)
  local copies, waits for them, and re-layouts  3.55 us (4%)
    pallas_call x1, Pallas kernels, body(): pl.pallas_call(functools.partial(moe_kernel, ep, tp_n, cap, heads), out_s...  85.9 us
    unnamed x2, local copies, waits for them, and re-layouts  3.55 us

profile of v3, /device:TPU:0, one launch (start us, length us, event | category | flops | bytes accessed | tf_op | source)
XLA Modules:
  0.0 90.1 jit_solution(10056100656797775427)
XLA Ops:
  0.6 85.9 %layer.1 = (bf16[64,2048]{1,0:T(8,128)(2,1)}, bf16[128,2048]{1,0:T(8,128)(2,1)}) custom-call(s32[2,128]{1,0:T(2,128)} %bitcast.7, f32[2,128]{1,0:T(2,128)} %bitcast.8, bf16[128,2048]{1,0:T(8,128)(2,1)} %tokens_ref.1, bf16[2048]{0:T(1024)(128)(2,1)} %gain_ref.1, bf16[256,2,128]{2,1,0:T(2,128)(2,1)} %q_ref.1, bf16[256,128]{1,0:T(8,128)(2,1)} %bitcast.5, ...), custom_call_target="tpu_custom_call" | custom-call | flops 9663676416 | bytes 6291456 | tf_op jit(solution)/shard_map/layer/pallas_call | solution.py:410
  86.6 1.7 %copy.16 = bf16[64,2048]{1,0:T(8,128)(2,1)} copy(bf16[64,2048]{1,0:T(8,128)(2,1)} %get-tuple-element.4) | data formatting | bytes 524288
  88.3 1.9 %copy.17 = bf16[128,2048]{1,0:T(8,128)(2,1)} copy(bf16[128,2048]{1,0:T(8,128)(2,1)} %get-tuple-element.5) | data formatting | bytes 1048576
